TPU v7x, 32 devices: a whole 2x2x4 slice. The times are simulated.
32 devices in a mesh: fs: 4 (over y, x), tp: 8 (over z, core).
Axes of the slice: x: 2, y: 2, z: 4, core: 2. Of those that a mesh axis runs over, the one named last changes fastest.
Arguments:
- saved_inputs: bfloat16 [2688, 4096], P('fs', 'tp'), may hold values from -6 to 6
- proj_cotangent: bfloat16 [2688, 4096], P('fs', 'tp'), may hold values from -0.115722656 to 0.115722656
- saved_hidden: bfloat16 [2688, 4096], P('fs', 'tp'), may hold values from -6 to 6
- out_cotangent: bfloat16 [2688, 4096], P('fs', 'tp'), may hold values from -0.115722656 to 0.115722656
- factors: bfloat16 [2, 4096, 128], replicated, may hold values from -0.46875 to 0.46875
- w_proj: float32 [4096, 4096], P('fs', 'tp'), may hold values from -0.09375 to 0.09375
- w_out: float32 [4096, 4096], P('tp', 'fs'), may hold values from -0.09375 to 0.09375
- moment_first: float32 [2, 128, 4096], P(None, None, 'tp'), may hold values from -1.8 to 1.8
- moment_second: float32 [2, 128, 4096], P(None, None, 'tp'), may hold values from 0.05 to 1
Outputs:
- proj_next: float32 [4096, 4096], P('fs', 'tp')
- out_next: float32 [4096, 4096], P('tp', 'fs')
- proj_copy: bfloat16 [4096, 4096], P(None, 'tp')
- out_copy: bfloat16 [4096, 4096], P('tp')
- first_next: float32 [2, 128, 4096], P(None, None, 'tp')
- second_next: float32 [2, 128, 4096], P(None, None, 'tp')
All inputs are finite; a program needn't handle non-finite values.
Results may differ from a plain program's by a relative error of at most 0.001.
Values may be sent and summed in bfloat16 or wider, within the bound.
A program may use at most 64 MiB of HBM per device.

v0:
```python
import jax
import jax.numpy as jnp
from jax import lax
from jax.sharding import PartitionSpec as P

beta_first = 0.9
beta_second = 0.95
learn_rate = 0.02
epsilon = 1e-06


def over_tokens(left_rows, right_rows, precise):
    return lax.dot_general(
        left_rows,
        right_rows,
        (((0,), (0,)), ((), ())),
        preferred_element_type=jnp.float32,
        precision=precise,
    )


def body(
    saved_inputs,
    proj_cotangent,
    saved_hidden,
    out_cotangent,
    factors,
    w_proj,
    w_out,
    moment_first,
    moment_second,
):
    highest = lax.Precision.HIGHEST
    fs_count = lax.axis_size("fs")
    tp_count = lax.axis_size("tp")
    d_model = factors.shape[1]
    hidden_width = proj_cotangent.shape[1]
    fs_rows = d_model // fs_count
    tp_feats = saved_inputs.shape[1]
    own_rows = lax.dynamic_slice_in_dim(factors, lax.axis_index("fs") * fs_rows, fs_rows, 1).astype(
        jnp.float32
    )
    own_feats = lax.dynamic_slice_in_dim(factors, lax.axis_index("tp") * tp_feats, tp_feats, 1)
    proj_rows = jnp.dot(saved_inputs, own_feats[0], preferred_element_type=jnp.float32)
    out_rows = jnp.dot(out_cotangent, own_feats[1], preferred_element_type=jnp.float32)
    proj_rows, out_rows = lax.psum((proj_rows, out_rows), "tp")
    partial_sums = jnp.stack(
        [
            over_tokens(proj_rows, proj_cotangent.astype(jnp.float32), highest),
            over_tokens(out_rows, saved_hidden.astype(jnp.float32), highest),
        ]
    )
    small_grads = lax.psum(partial_sums, "fs")
    first_next = beta_first * moment_first + (1.0 - beta_first) * small_grads
    second_next = beta_second * moment_second + (1.0 - beta_second) * small_grads * small_grads
    direction = first_next / (jnp.sqrt(second_next) + epsilon)
    update_full = jnp.einsum("kdr,kre->kde", own_rows, direction, precision=highest)
    squares = lax.psum(jnp.sum(update_full * update_full, axis=(1, 2)), ("fs", "tp"))
    norm_scale = lax.rsqrt(squares / (d_model * hidden_width * tp_count) + epsilon)
    stepped = update_full * norm_scale[:, None, None]
    proj_next = w_proj - learn_rate * stepped[0]
    out_next = w_out - learn_rate * stepped[1].T
    proj_copy, out_copy = (
        lax.all_gather(proj_next.astype(jnp.bfloat16), "fs", axis=0, tiled=True),
        lax.all_gather(out_next.astype(jnp.bfloat16), "fs", axis=1, tiled=True),
    )
    return (proj_next, out_next, proj_copy, out_copy, first_next, second_next)


def solution(mesh):
    placed = (
        P("fs", "tp"),
        P("fs", "tp"),
        P("fs", "tp"),
        P("fs", "tp"),
        P(),
        P("fs", "tp"),
        P("tp", "fs"),
        P(None, None, "tp"),
        P(None, None, "tp"),
    )
    return jax.shard_map(
        body,
        mesh=mesh,
        in_specs=placed,
        out_specs=(
            P("fs", "tp"),
            P("tp", "fs"),
            P(None, "tp"),
            P("tp", None),
            P(None, None, "tp"),
            P(None, None, "tp"),
        ),
        check_vma=False,
    )
```

profile of v0, /device:TPU:0, one launch (start us, length us, event | category | flops | bytes accessed | tf_op | source)
XLA Modules:
  0.0 292.3 jit_solution(14841451723777137700)
XLA Ops:
  7.2 0.0 copy-start
  7.2 0.0 all-reduce.6.cloned.1.call-start
  7.2 1.5 copy-done
  8.8 2.3 convolution_bitcast_fusion.1
  11.1 2.2 convolution_bitcast_fusion
  13.3 0.0 all-reduce.6.cloned.1.call-update
  13.3 0.0 all-reduce.4.cloned.1.call-start
  13.3 60.8 %all-reduce.6.cloned.1.call-done = (f32[672,128]{0,1:T(8,128)}, f32[672,128]{0,1:T(8,128)}) async-done(((f32[672,128]{0,1:T(8,128)}, f32[672,128]{0,1:T(8,128)}), (f32[672,128]{0,1:T(8,128)}, f32[672,128]{0,1:T(8,128)})) %all-reduce.6.cloned.1.call-update) | async-done | bytes 688144 | tf_op jit(solution)/shard_map/psum | solution.py:46
  74.1 1.5 convolution_bitcast_fusion.2
  75.6 1.5 convolution_bitcast_fusion.3
  77.1 0.8 pad_maximum_fusion
  77.9 0.0 all-reduce.4.cloned.1.call-update
  77.9 0.0 all-gather.5.cloned.1.call-start
  78.0 2.9 copy.15
  80.9 41.7 %all-reduce.4.cloned.1.call-done = f32[2,128,512]{2,1,0:T(8,128)} async-done(((f32[2,128,512]{2,1,0:T(8,128)}), f32[2,128,512]{2,1,0:T(8,128)}) %all-reduce.4.cloned.1.call-update) | async-done | bytes 524304 | tf_op jit(solution)/shard_map/psum | solution.py:53
  122.6 1.6 fusion.4
  124.2 0.0 copy-start.3
  124.2 0.0 copy-start.4
  124.2 4.0 %multiply_reduce_fusion = (f32[2]{0:T(128)S(1)}, f32[2,1024,512]{2,1,0:T(8,128)}) fusion(f32[2,128,512]{2,1,0:T(8,128)S(1)} %get-tuple-element.32, f32[2,128,512]{2,1,0:T(8,128)S(1)} %get-tuple-element.33, bf16[2,4096,128]{2,1,0:T(8,128)(2,1)S(1)} %copy-done, s32[]{:T(128)S(6)} %select_n.6), kind=kOutput, calls=%fused_computation | convolution fusion | flops 1612972032 | bytes 5767180 | tf_op jit(solution)/shard_map/kdr,kre->kde/dot_general | solution.py:57
  128.2 39.2 %psum.31 = f32[2]{0:T(128)S(1)} all-reduce(f32[2]{0:T(128)S(1)} %get-tuple-element.20), channel_id=1, replica_groups=mesh['fs'=4,'tp'=8] {'fs','tp'}, use_global_device_ids=true, to_apply=%region_4.0 | all-reduce | flops 2 | bytes 16 | tf_op jit(solution)/shard_map/psum | solution.py:58
  167.4 3.1 %broadcast_multiply_fusion = f32[2,1024,512]{2,1,0:T(8,128)S(1)} fusion(f32[2,1024,512]{2,1,0:T(8,128)} %get-tuple-element.21, f32[2]{0:T(128)S(1)} %add_rsqrt_fusion), kind=kLoop, calls=%fused_computation.7 | loop fusion | flops 1048576 | bytes 8388616 | tf_op jit(solution)/shard_map/mul | solution.py:60
  170.6 2.6 fusion.15
  173.2 0.4 copy-done.1
  173.5 0.0 all-gather.5.cloned.1.call-update
  173.6 0.0 all-gather.3.cloned.1.call-start
  173.6 4.5 %fusion.17 = (bf16[1024,512]{1,0:T(8,128)(2,1)}, f32[1024,512]{1,0:T(8,128)}) fusion(f32[1024,512]{1,0:T(8,128)} %param.14, f32[2,1024,512]{2,1,0:T(8,128)} %copy-done.1), kind=kLoop, calls=%fused_computation.30 | loop fusion | flops 1572864 | bytes 7340032 | tf_op jit(solution)/shard_map/convert_element_type | solution.py:64
  178.1 0.0 all-gather.3.cloned.1.call-update
  178.1 2.9 copy.16
  181.0 46.0 %all-gather.5.cloned.1.call-done = bf16[512,4096]{0,1:T(8,128)(2,1)} async-done(((bf16[512,1024]{0,1:T(8,128)(2,1)}), bf16[512,4096]{0,1:T(8,128)(2,1)}) %all-gather.5.cloned.1.call-update) | async-done | bytes 4194320 | tf_op jit(solution)/shard_map/all_gather | solution.py:65
  227.0 6.3 %copy.17 = bf16[512,4096]{1,0:T(8,128)(2,1)} copy(bf16[512,4096]{0,1:T(8,128)(2,1)} %all-gather.5.cloned.1.call-done) | data formatting | bytes 8388608
  233.3 48.0 %all-gather.3.cloned.1.call-done = bf16[4096,512]{1,0:T(8,128)(2,1)} async-done(((bf16[1024,512]{1,0:T(8,128)(2,1)}), bf16[4096,512]{1,0:T(8,128)(2,1)}) %all-gather.3.cloned.1.call-update) | async-done | bytes 4194320 | tf_op jit(solution)/shard_map/all_gather | solution.py:64
  281.3 4.5 %copy.22 = bf16[4096,512]{1,0:T(8,128)(2,1)} copy(bf16[4096,512]{1,0:T(8,128)(2,1)} %all-gather.3.cloned.1.call-done) | data formatting | bytes 8388608
  (10 shorter events, 0.0 us)
Async XLA Ops:
  7.2 1.6 copy-start
  7.2 66.9 %copy-start.5 = (bf16[672,512]{1,0:T(8,128)(2,1)S(1)}, bf16[672,512]{1,0:T(8,128)(2,1)}, u32[]{:S(2)}) copy-start(bf16[672,512]{1,0:T(8,128)(2,1)} %param.11) | copy-start | bytes 2064388
  7.2 66.9 %all-reduce.6.cloned.1.call-start = ((), (), s32[]{:S(2)}) async-start(), calls=%async_computation.3 | async-start | bytes 1572864 | tf_op jit(solution)/shard_map/psum | solution.py:46
  8.8 66.8 %copy-start.6 = (bf16[672,512]{1,0:T(8,128)(2,1)S(1)}, bf16[672,512]{1,0:T(8,128)(2,1)}, u32[]{:S(2)}) copy-start(bf16[672,512]{1,0:T(8,128)(2,1)} %param.10) | copy-start | bytes 2064388
  13.3 109.3 %all-reduce.4.cloned.1.call-start = ((), (), s32[]{:S(2)}) async-start(), calls=%async_computation | async-start | bytes 1048576 | tf_op jit(solution)/shard_map/psum | solution.py:53
  77.9 149.1 %all-gather.5.cloned.1.call-start = ((), (), s32[]{:S(2)}) async-start(), calls=%async_computation.2 | async-start | bytes 5242880 | tf_op jit(solution)/shard_map/all_gather | solution.py:65
  124.2 4.0 %copy-start.3 = (f32[2,128,512]{2,1,0:T(8,128)}, f32[2,128,512]{2,1,0:T(8,128)S(1)}, u32[]{:S(2)}) copy-start(f32[2,128,512]{2,1,0:T(8,128)S(1)} %get-tuple-element.33) | copy-start | bytes 1572868
  124.2 4.0 %copy-start.4 = (f32[2,128,512]{2,1,0:T(8,128)}, f32[2,128,512]{2,1,0:T(8,128)S(1)}, u32[]{:S(2)}) copy-start(f32[2,128,512]{2,1,0:T(8,128)S(1)} %get-tuple-element.32) | copy-start | bytes 1572868
  167.4 3.1 %copy-start.2 = (f32[512,1024]{0,1:T(8,128)S(1)}, f32[512,1024]{0,1:T(8,128)}, u32[]{:S(2)}) copy-start(f32[512,1024]{0,1:T(8,128)} %copy.15) | copy-start | bytes 6291460
  170.6 3.0 %copy-start.1 = (f32[2,1024,512]{2,1,0:T(8,128)}, f32[2,1024,512]{2,1,0:T(8,128)S(1)}, u32[]{:S(2)}) copy-start(f32[2,1024,512]{2,1,0:T(8,128)S(1)} %broadcast_multiply_fusion) | copy-start | bytes 12582916
  173.6 107.8 %all-gather.3.cloned.1.call-start = ((), (), s32[]{:S(2)}) async-start(), calls=%async_computation.1 | async-start | bytes 5242880 | tf_op jit(solution)/shard_map/all_gather | solution.py:64
Sparse Core Ops, SparseCore 0:
  13.4 60.6 all-reduce.5
  78.1 44.4 all-reduce.3
  173.7 53.2 all-gather.4
  228.7 52.5 all-gather.2
where the time goes:
time: 293 us; the launch traced here: 292 us
  waiting for transfers between devices  197 us (67%)
  blocking collectives  39.2 us (13%)
  local copies, waits for them, and re-layouts  18.5 us (6%)
  between operations  13.9 us (5%)
  other arithmetic  12.6 us (4%)
  matrix products  11.4 us (4%)
    psum x1, waiting for transfers between devices, body(): proj_rows, out_rows = lax.psum((proj_rows, out_rows), 'tp')  60.8 us
    all_gather x1, waiting for transfers between devices, body(): lax.all_gather(proj_next.astype(jnp.bfloat16), 'fs', axis=0, tiled=True)  48 us
    all_gather x1, waiting for transfers between devices, body(): lax.all_gather(out_next.astype(jnp.bfloat16), 'fs', axis=1, tiled=True)  46 us
    psum x1, waiting for transfers between devices, body(): small_grads = lax.psum(partial_sums, 'fs')  41.7 us
    psum x1, blocking collectives, body(): lax.psum(jnp.sum(update_full * update_full, axis=(1, 2)), ('fs', 'tp'))  39.2 us
    unnamed x18, local copies, waits for them, and re-layouts  18.5 us
  transfers between devices with their start and end apart: 4, of which 4 were waited for; matrix products, arithmetic and copies ran while one was open for 6% of the time, Pallas kernels for 0%

commit v1 on v0

--- a/solution.py
+++ b/solution.py
@@ -7,6 +7,15 @@
 beta_second = 0.95
 learn_rate = 0.02
 epsilon = 1e-06
+
+
+def added_up(x, axis):
+    peers = lax.axis_size(axis)
+    result, far = (x, 1)
+    while far < peers:
+        result = result + lax.ppermute(result, axis, [(i, i ^ far) for i in range(peers)])
+        far = 2 * far
+    return result
 
 
 def over_tokens(left_rows, right_rows, precise):
@@ -50,7 +59,7 @@
             over_tokens(out_rows, saved_hidden.astype(jnp.float32), highest),
         ]
     )
-    small_grads = lax.psum(partial_sums, "fs")
+    small_grads = added_up(partial_sums, "fs")
     first_next = beta_first * moment_first + (1.0 - beta_first) * small_grads
     second_next = beta_second * moment_second + (1.0 - beta_second) * small_grads * small_grads
     direction = first_next / (jnp.sqrt(second_next) + epsilon)

time: 293 us -> 272 us (0.928)
  waiting for transfers between devices: 197 us -> 171 us
  starting transfers between devices: 0.16 us -> 3.2 us
    psum x1 -> x0, waiting for transfers between devices: 41.7 us -> none  [body(): small_grads = lax.psum(partial_sums, 'fs')]
    ppermute x0 -> x2, waiting for transfers between devices: none -> 17.3 us  [added_up(): lax.ppermute(result, axis, [(i, i ^ far) for i in range(peers)])]
    ppermute x0 -> x2, starting transfers between devices: none -> 3.08 us  [added_up(): lax.ppermute(result, axis, [(i, i ^ far) for i in range(peers)])]
  transfers between devices with their start and end apart: 4 -> 5, of which waited for: 4 -> 5; matrix products, arithmetic and copies ran while one was open for 6% -> 6% of each run, Pallas kernels for 0% -> 0%
where the time goes in v1:
time: 272 us; the launch traced here: 271 us
  waiting for transfers between devices  171 us (63%)
  blocking collectives  39.7 us (15%)
  local copies, waits for them, and re-layouts  19.3 us (7%)
  between operations  13.8 us (5%)
  other arithmetic  12.2 us (4%)
  matrix products  11.6 us (4%)
  starting transfers between devices  3.2 us (1%)
    psum x1, waiting for transfers between devices, body(): proj_rows, out_rows = lax.psum((proj_rows, out_rows), 'tp')  60.7 us
    all_gather x1, waiting for transfers between devices, body(): lax.all_gather(proj_next.astype(jnp.bfloat16), 'fs', axis=0, tiled=True)  48.1 us
    all_gather x1, waiting for transfers between devices, body(): lax.all_gather(out_next.astype(jnp.bfloat16), 'fs', axis=1, tiled=True)  45.2 us
    psum x1, blocking collectives, body(): lax.psum(jnp.sum(update_full * update_full, axis=(1, 2)), ('fs', 'tp'))  39.7 us
    unnamed x18, local copies, waits for them, and re-layouts  19.3 us
    ppermute x2, waiting for transfers between devices, added_up(): lax.ppermute(result, axis, [(i, i ^ far) for i in range(peers)])  17.3 us
  transfers between devices with their start and end apart: 5, of which 5 were waited for; matrix products, arithmetic and copies ran while one was open for 6% of the time, Pallas kernels for 0%

profile of v1, /device:TPU:0, one launch (start us, length us, event | category | flops | bytes accessed | tf_op | source)
XLA Modules:
  0.0 271.3 jit_solution(4816166301081543648)
XLA Ops:
  7.2 0.0 copy-start
  7.2 0.0 all-reduce.3.cloned.1.call-start
  7.2 1.5 copy-done
  8.8 2.2 convolution_bitcast_fusion.1
  11.0 2.2 convolution_bitcast_fusion
  13.2 0.0 all-reduce.3.cloned.1.call-update
  13.2 0.0 all-gather.5.cloned.1.call-start
  13.3 60.7 %all-reduce.3.cloned.1.call-done = (f32[672,128]{0,1:T(8,128)}, f32[672,128]{0,1:T(8,128)}) async-done(((f32[672,128]{0,1:T(8,128)}, f32[672,128]{0,1:T(8,128)}), (f32[672,128]{0,1:T(8,128)}, f32[672,128]{0,1:T(8,128)})) %all-reduce.3.cloned.1.call-update) | async-done | bytes 688144 | tf_op jit(solution)/shard_map/psum | solution.py:55
  74.0 1.5 convolution_bitcast_fusion.2
  75.5 1.7 convolution_bitcast_fusion.3
  77.2 1.5 collective-permute-start
  78.8 10.5 %collective-permute-done = f32[2,128,512]{2,1,0:T(8,128)S(1)} collective-permute-done((f32[2,128,512]{2,1,0:T(8,128)S(1)}, f32[2,128,512]{2,1,0:T(8,128)S(1)}, u32[]{:S(2)}, u32[]{:S(2)}) %collective-permute-start) | collective-permute-done | bytes 524320 | tf_op jit(solution)/shard_map/ppermute | solution.py:16
  89.3 0.8 copy-done.5
  90.0 0.1 fusion.15
  90.1 1.5 collective-permute-start.1
  91.7 2.9 %copy.15 = f32[512,1024]{0,1:T(8,128)} copy(f32[512,1024]{1,0:T(8,128)} %param.15) | data formatting | bytes 4194304 | tf_op args[6]
  94.6 6.8 %collective-permute-done.1 = f32[2,128,512]{2,1,0:T(8,128)} collective-permute-done((f32[2,128,512]{2,1,0:T(8,128)S(1)}, f32[2,128,512]{2,1,0:T(8,128)}, u32[]{:S(2)}, u32[]{:S(2)}) %collective-permute-start.1) | collective-permute-done | bytes 524320 | tf_op jit(solution)/shard_map/ppermute | solution.py:16
  101.4 1.8 fusion.4
  103.3 4.0 %multiply_reduce_fusion = (f32[2]{0:T(128)S(1)}, f32[2,1024,512]{2,1,0:T(8,128)}) fusion(f32[2,128,512]{2,1,0:T(8,128)S(1)} %get-tuple-element.32, f32[2,128,512]{2,1,0:T(8,128)S(1)} %get-tuple-element.33, bf16[2,4096,128]{2,1,0:T(8,128)(2,1)S(1)} %copy-done, s32[]{:T(128)S(6)} %select_n.6), kind=kOutput, calls=%fused_computation | convolution fusion | flops 1612972032 | bytes 5767180 | tf_op jit(solution)/shard_map/kdr,kre->kde/dot_general | solution.py:66
  107.3 39.7 %psum.23 = f32[2]{0:T(128)S(1)} all-reduce(f32[2]{0:T(128)S(1)} %get-tuple-element.20), channel_id=1, replica_groups=mesh['fs'=4,'tp'=8] {'fs','tp'}, use_global_device_ids=true, to_apply=%region_3.0 | all-reduce | flops 2 | bytes 16 | tf_op jit(solution)/shard_map/psum | solution.py:67
  147.0 3.1 %broadcast_multiply_fusion = f32[2,1024,512]{2,1,0:T(8,128)S(1)} fusion(f32[2,1024,512]{2,1,0:T(8,128)} %get-tuple-element.21, f32[2]{0:T(128)S(1)} %add_rsqrt_fusion), kind=kLoop, calls=%fused_computation.7 | loop fusion | flops 1048576 | bytes 8388616 | tf_op jit(solution)/shard_map/mul | solution.py:69
  150.2 2.6 fusion.16
  152.7 0.4 copy-done.1
  153.1 0.0 all-gather.5.cloned.1.call-update
  153.1 0.0 all-gather.3.cloned.1.call-start
  153.2 4.5 %fusion.18 = (bf16[1024,512]{1,0:T(8,128)(2,1)}, f32[1024,512]{1,0:T(8,128)}) fusion(f32[1024,512]{1,0:T(8,128)} %param.14, f32[2,1024,512]{2,1,0:T(8,128)} %copy-done.1), kind=kLoop, calls=%fused_computation.31 | loop fusion | flops 1572864 | bytes 7340032 | tf_op jit(solution)/shard_map/convert_element_type | solution.py:73
  157.7 0.0 all-gather.3.cloned.1.call-update
  157.7 2.9 %copy.16 = f32[512,1024]{1,0:T(8,128)} copy(f32[512,1024]{0,1:T(8,128)} %get-tuple-element.15) | data formatting | bytes 4194304
  160.6 45.2 %all-gather.5.cloned.1.call-done = bf16[512,4096]{0,1:T(8,128)(2,1)} async-done(((bf16[512,1024]{0,1:T(8,128)(2,1)}), bf16[512,4096]{0,1:T(8,128)(2,1)}) %all-gather.5.cloned.1.call-update) | async-done | bytes 4194320 | tf_op jit(solution)/shard_map/all_gather | solution.py:74
  205.8 6.3 %copy.17 = bf16[512,4096]{1,0:T(8,128)(2,1)} copy(bf16[512,4096]{0,1:T(8,128)(2,1)} %all-gather.5.cloned.1.call-done) | data formatting | bytes 8388608
  212.1 48.1 %all-gather.3.cloned.1.call-done = bf16[4096,512]{1,0:T(8,128)(2,1)} async-done(((bf16[1024,512]{1,0:T(8,128)(2,1)}), bf16[4096,512]{1,0:T(8,128)(2,1)}) %all-gather.3.cloned.1.call-update) | async-done | bytes 4194320 | tf_op jit(solution)/shard_map/all_gather | solution.py:73
  260.3 4.5 %copy.21 = bf16[4096,512]{1,0:T(8,128)(2,1)} copy(bf16[4096,512]{1,0:T(8,128)(2,1)} %all-gather.3.cloned.1.call-done) | data formatting | bytes 8388608
  (12 shorter events, 0.1 us)
Async XLA Ops:
  7.2 1.6 copy-start
  7.2 66.8 %copy-start.6 = (bf16[672,512]{1,0:T(8,128)(2,1)S(1)}, bf16[672,512]{1,0:T(8,128)(2,1)}, u32[]{:S(2)}) copy-start(bf16[672,512]{1,0:T(8,128)(2,1)} %param.11) | copy-start | bytes 2064388
  7.2 66.8 %all-reduce.3.cloned.1.call-start = ((), (), s32[]{:S(2)}) async-start(), calls=%async_computation.2 | async-start | bytes 1572864 | tf_op jit(solution)/shard_map/psum | solution.py:55
  13.2 192.6 %all-gather.5.cloned.1.call-start = ((), (), s32[]{:S(2)}) async-start(), calls=%async_computation.1 | async-start | bytes 5242880 | tf_op jit(solution)/shard_map/all_gather | solution.py:74
  77.2 12.0 %collective-permute-start = (f32[2,128,512]{2,1,0:T(8,128)S(1)}, f32[2,128,512]{2,1,0:T(8,128)S(1)}, u32[]{:S(2)}, u32[]{:S(2)}) collective-permute-start(f32[2,128,512]{2,1,0:T(8,128)S(1)} %pad_maximum_fusion), channel_id=1, source_target_pairs={{0,8},{8,0},{16,24},{24,16},{1,9},{9,1},{17,25},{25,17},{2,10},{10... | collective-permute-start | bytes 1572872 | tf_op jit(solution)/shard_map/ppermute | solution.py:16
  89.3 0.8 copy-start.5
  90.1 11.3 %collective-permute-start.1 = (f32[2,128,512]{2,1,0:T(8,128)S(1)}, f32[2,128,512]{2,1,0:T(8,128)}, u32[]{:S(2)}, u32[]{:S(2)}) collective-permute-start(f32[2,128,512]{2,1,0:T(8,128)S(1)} %fusion.15), channel_id=1, source_target_pairs={{0,16},{8,24},{16,0},{24,8},{1,17},{9,25},{17,1},{25,9},{2,18},{10... | collective-permute-start | bytes 1572872 | tf_op jit(solution)/shard_map/ppermute | solution.py:16
  103.2 4.0 %copy-start.3 = (f32[2,128,512]{2,1,0:T(8,128)}, f32[2,128,512]{2,1,0:T(8,128)S(1)}, u32[]{:S(2)}) copy-start(f32[2,128,512]{2,1,0:T(8,128)S(1)} %get-tuple-element.33) | copy-start | bytes 1572868
  103.3 4.0 %copy-start.4 = (f32[2,128,512]{2,1,0:T(8,128)}, f32[2,128,512]{2,1,0:T(8,128)S(1)}, u32[]{:S(2)}) copy-start(f32[2,128,512]{2,1,0:T(8,128)S(1)} %get-tuple-element.32) | copy-start | bytes 1572868
  147.0 3.1 %copy-start.2 = (f32[512,1024]{0,1:T(8,128)S(1)}, f32[512,1024]{0,1:T(8,128)}, u32[]{:S(2)}) copy-start(f32[512,1024]{0,1:T(8,128)} %copy.15) | copy-start | bytes 6291460
  150.2 3.0 %copy-start.1 = (f32[2,1024,512]{2,1,0:T(8,128)}, f32[2,1024,512]{2,1,0:T(8,128)S(1)}, u32[]{:S(2)}) copy-start(f32[2,1024,512]{2,1,0:T(8,128)S(1)} %broadcast_multiply_fusion) | copy-start | bytes 12582916
  153.1 107.1 %all-gather.3.cloned.1.call-start = ((), (), s32[]{:S(2)}) async-start(), calls=%async_computation | async-start | bytes 5242880 | tf_op jit(solution)/shard_map/all_gather | solution.py:73
Sparse Core Ops, SparseCore 0:
  13.3 60.6 all-reduce.2
  153.3 52.4 all-gather.4
  207.7 52.5 all-gather.2
